TPU v7x, 32 devices: a whole 2x2x4 slice. The times are simulated.
32 devices in a mesh: fs: 8 (over z, x), tp: 4 (over y, core).
Axes of the slice: x: 2, y: 2, z: 4, core: 2. Of those that a mesh axis runs over, the one named last changes fastest.
Arguments:
- prompts: bfloat16 [4, 1024, 2048], P('tp'), may hold values from -6 to 6
- gain_first: float32 [2048], P('fs'), may hold values from 0.1 to 1.9
- gate_first: float32 [2048, 5632], P('fs', 'tp'), may hold values from -0.125 to 0.125
- up_first: float32 [2048, 5632], P('fs', 'tp'), may hold values from -0.125 to 0.125
- down_first: float32 [5632, 2048], P('fs', 'tp'), may hold values from -0.078125 to 0.078125
- gain_second: float32 [2048], P('fs'), may hold values from 0.1 to 1.9
- gate_second: float32 [2048, 5632], P('fs', 'tp'), may hold values from -0.125 to 0.125
- up_second: float32 [2048, 5632], P('fs', 'tp'), may hold values from -0.125 to 0.125
- down_second: float32 [5632, 2048], P('fs', 'tp'), may hold values from -0.078125 to 0.078125
Outputs:
- served_gate_first: bfloat16 [2048, 5632], P(None, 'fs')
- served_up_first: bfloat16 [2048, 5632], P(None, 'fs')
- served_down_first: bfloat16 [5632, 2048], P('fs')
- served_gate_second: bfloat16 [2048, 5632], P(None, 'fs')
- served_up_second: bfloat16 [2048, 5632], P(None, 'fs')
- served_down_second: bfloat16 [5632, 2048], P('fs')
- prompt_states: bfloat16 [4, 1024, 2048], P('tp', 'fs')
All inputs are finite; a program needn't handle non-finite values.
Results may differ from a plain program's by a relative error of at most 0.012.
Values may be sent and summed in bfloat16 or wider, within the bound.
A program may use at most 128 MiB of HBM per device.

v0:
```python
import jax
import jax.numpy as jnp
from jax import lax
from jax.sharding import PartitionSpec as P


def normalize(row_block):
    widened = row_block.astype(jnp.float32)
    scaled = widened * lax.rsqrt(jnp.mean(widened * widened, axis=-1, keepdims=True) + 1e-06)
    return scaled.astype(jnp.bfloat16)


def activate(normed, gate_cols, up_cols):
    gate_val = jnp.dot(normed, gate_cols, preferred_element_type=jnp.float32)
    up_val = jnp.dot(normed, up_cols, preferred_element_type=jnp.float32)
    return (jax.nn.silu(gate_val) * up_val).astype(jnp.bfloat16)


def reorder(matrix, outer_count, inner_count):
    total_rows, columns = matrix.shape
    block_rows = total_rows // (outer_count * inner_count)
    shaped = matrix.reshape(outer_count, inner_count, block_rows, columns)
    return jnp.transpose(shaped, (1, 0, 2, 3)).reshape(total_rows, columns)


def per_device(
    prompts,
    gain_first,
    gate_first,
    up_first,
    down_first,
    gain_second,
    gate_second,
    up_second,
    down_second,
):
    fold_gate_a = (gain_first[:, None] * gate_first).astype(jnp.bfloat16)
    fold_up_a = (gain_first[:, None] * up_first).astype(jnp.bfloat16)
    fold_gate_b = (gain_second[:, None] * gate_second).astype(jnp.bfloat16)
    fold_up_b = (gain_second[:, None] * up_second).astype(jnp.bfloat16)
    round_down_a = down_first.astype(jnp.bfloat16)
    round_down_b = down_second.astype(jnp.bfloat16)
    sliced = (
        lax.all_to_all(fold_gate_a, "tp", split_axis=0, concat_axis=1, tiled=True),
        lax.all_to_all(fold_up_a, "tp", split_axis=0, concat_axis=1, tiled=True),
        lax.all_to_all(fold_gate_b, "tp", split_axis=0, concat_axis=1, tiled=True),
        lax.all_to_all(fold_up_b, "tp", split_axis=0, concat_axis=1, tiled=True),
    )
    blocked = (
        lax.all_to_all(sliced[0], "fs", split_axis=1, concat_axis=0, tiled=True),
        lax.all_to_all(sliced[1], "fs", split_axis=1, concat_axis=0, tiled=True),
        lax.all_to_all(sliced[2], "fs", split_axis=1, concat_axis=0, tiled=True),
        lax.all_to_all(sliced[3], "fs", split_axis=1, concat_axis=0, tiled=True),
    )
    collected = (
        lax.all_gather(blocked[0], "tp", axis=0, tiled=True),
        lax.all_gather(blocked[1], "tp", axis=0, tiled=True),
        lax.all_gather(blocked[2], "tp", axis=0, tiled=True),
        lax.all_gather(blocked[3], "tp", axis=0, tiled=True),
    )
    outer_count = lax.axis_size("tp")
    inner_count = lax.axis_size("fs")
    gate_a = reorder(collected[0], outer_count, inner_count)
    up_a = reorder(collected[1], outer_count, inner_count)
    gate_b = reorder(collected[2], outer_count, inner_count)
    up_b = reorder(collected[3], outer_count, inner_count)
    down_a, down_b = (
        lax.all_gather(round_down_a, "tp", axis=1, tiled=True),
        lax.all_gather(round_down_b, "tp", axis=1, tiled=True),
    )
    tokens_in = prompts.reshape(-1, prompts.shape[-1])
    share = tokens_in.shape[0] // lax.axis_size("fs")
    act_first = activate(normalize(tokens_in), gate_a, up_a)
    selected = act_first
    summed = lax.psum_scatter(
        jnp.dot(selected, down_a, preferred_element_type=jnp.float32).astype(jnp.bfloat16),
        "fs",
        scatter_dimension=0,
        tiled=True,
    ).astype(jnp.float32)
    own_rows = lax.dynamic_slice_in_dim(tokens_in, lax.axis_index("fs") * share, share, 0)
    middle = (own_rows.astype(jnp.float32) + 0.5 * summed).astype(jnp.bfloat16)
    act_second = activate(lax.all_gather(normalize(middle), "fs", axis=0, tiled=True), gate_b, up_b)
    selected = act_second
    final_sum = lax.psum_scatter(
        jnp.dot(selected, down_b, preferred_element_type=jnp.float32).astype(jnp.bfloat16),
        "fs",
        scatter_dimension=0,
        tiled=True,
    ).astype(jnp.float32)
    finished = (middle.astype(jnp.float32) + 0.5 * final_sum).astype(jnp.bfloat16)
    return (
        gate_a,
        up_a,
        down_a,
        gate_b,
        up_b,
        down_b,
        finished.reshape(prompts.shape[0], share, prompts.shape[-1]),
    )


def solution(mesh):
    in_specs = (
        P("tp", None, None),
        P("fs"),
        P("fs", "tp"),
        P("fs", "tp"),
        P("fs", "tp"),
        P("fs"),
        P("fs", "tp"),
        P("fs", "tp"),
        P("fs", "tp"),
    )
    out_specs = (
        P(None, "fs"),
        P(None, "fs"),
        P("fs", None),
        P(None, "fs"),
        P(None, "fs"),
        P("fs", None),
        P("tp", "fs", None),
    )
    return jax.shard_map(
        per_device, mesh=mesh, in_specs=in_specs, out_specs=out_specs, check_vma=False
    )
```

profile of v0, /device:TPU:0, one launch (start us, length us, event | category | flops | bytes accessed | tf_op | source)
XLA Modules:
  0.0 561.2 jit_solution(2317630141392950479)
XLA Ops:
  9.3 15.0 %all_to_all.140 = bf16[4,64,1408]{2,1,0:T(8,128)(2,1)S(1)} all-to-all(bf16[4,64,1408]{2,1,0:T(8,128)(2,1)S(1)} %bitcast.74), channel_id=1, replica_groups=mesh['fs'=8,'tp'=4] {'tp'}, dimensions={0} | all-to-all | bytes 1441792 | tf_op jit(solution)/shard_map/all_to_all | solution.py:44
  25.5 25.8 %all_to_all.141 = bf16[64,8,704]{2,0,1:T(8,128)(2,1)} all-to-all(bf16[64,8,704]{2,0,1:T(8,128)(2,1)S(1)} %copy.33), channel_id=1, replica_groups=mesh['fs'=8,'tp'=4] {'fs'}, dimensions={1} | all-to-all | bytes 1441792 | tf_op jit(solution)/shard_map/all_to_all | solution.py:50
  51.3 18.9 %all_to_all.142 = bf16[4,64,1408]{2,1,0:T(8,128)(2,1)S(1)} all-to-all(bf16[4,64,1408]{2,1,0:T(8,128)(2,1)S(1)} %bitcast.72), channel_id=1, replica_groups=mesh['fs'=8,'tp'=4] {'tp'}, dimensions={0} | all-to-all | bytes 1441792 | tf_op jit(solution)/shard_map/all_to_all | solution.py:45
  71.4 23.3 %all_to_all.143 = bf16[64,8,704]{2,0,1:T(8,128)(2,1)} all-to-all(bf16[64,8,704]{2,0,1:T(8,128)(2,1)S(1)} %copy.36), channel_id=1, replica_groups=mesh['fs'=8,'tp'=4] {'fs'}, dimensions={1} | all-to-all | bytes 1441792 | tf_op jit(solution)/shard_map/all_to_all | solution.py:51
  95.8 3.1 fusion
  98.9 2.5 copy.34
  101.4 20.1 %all-gather.10.cloned.1.call-done = bf16[2048,704]{1,0:T(8,128)(2,1)} async-done(((bf16[512,704]{1,0:T(8,128)(2,1)}), bf16[2048,704]{1,0:T(8,128)(2,1)}) %all-gather.10.cloned.1.call-update) | async-done | bytes 2883600 | tf_op jit(solution)/shard_map/all_gather | solution.py:57
  121.5 4.1 copy.37
  125.6 5.0 fusion.4
  130.6 20.1 %all-gather.12.cloned.1.call-done = bf16[704,2048]{1,0:T(8,128)(2,1)} async-done(((bf16[704,512]{1,0:T(8,128)(2,1)}), bf16[704,2048]{1,0:T(8,128)(2,1)}) %all-gather.12.cloned.1.call-update) | async-done | bytes 2883600 | tf_op jit(solution)/shard_map/all_gather | solution.py:68
  150.7 12.6 %convolution_convert_fusion.1 = bf16[1024,2048]{1,0:T(8,128)(2,1)} fusion(bf16[704,2048]{1,0:T(8,128)(2,1)} %all-gather.12.cloned.1.call-done, f32[1024,704]{0,1:T(8,128)} %fusion.4, bf16[2048,704]{1,0:T(8,128)(2,1)} %bitcast.58, bf16[1,1024,2048]{2,1,0:T(8,128)(2,1)} %param.9, f32[1024]{0:T(1024)S(1)} %add_rsqrt_fusion), kind=kOutput, calls=%fused_computation.6 | convolution fusion | flops 5918294016 | bytes 17043456 | tf_op jit(solution)/shard_map/dot_general | solution.py:76
  164.0 2.9 multiply_convert_fusion.2
  166.9 13.3 %all_to_all.144 = bf16[4,64,1408]{2,1,0:T(8,128)(2,1)S(1)} all-to-all(bf16[4,64,1408]{2,1,0:T(8,128)(2,1)S(1)} %bitcast.75), channel_id=1, replica_groups=mesh['fs'=8,'tp'=4] {'tp'}, dimensions={0} | all-to-all | bytes 1441792 | tf_op jit(solution)/shard_map/all_to_all | solution.py:46
  181.6 2.4 all_to_all.121
  185.3 38.9 %all_to_all.145 = bf16[64,8,704]{2,0,1:T(8,128)(2,1)} all-to-all(bf16[64,8,704]{2,0,1:T(8,128)(2,1)S(1)} %copy.39), channel_id=1, replica_groups=mesh['fs'=8,'tp'=4] {'fs'}, dimensions={1} | all-to-all | bytes 1441792 | tf_op jit(solution)/shard_map/all_to_all | solution.py:52
  224.3 14.4 %all_to_all.146 = bf16[4,64,1408]{2,1,0:T(8,128)(2,1)S(1)} all-to-all(bf16[4,64,1408]{2,1,0:T(8,128)(2,1)} %bitcast.73), channel_id=1, replica_groups=mesh['fs'=8,'tp'=4] {'tp'}, dimensions={0} | all-to-all | bytes 1441792 | tf_op jit(solution)/shard_map/all_to_all | solution.py:47
  240.1 2.4 all_to_all.128
  243.8 39.6 %all_to_all.147 = bf16[64,8,704]{2,0,1:T(8,128)(2,1)} all-to-all(bf16[64,8,704]{2,0,1:T(8,128)(2,1)S(1)} %copy.42), channel_id=1, replica_groups=mesh['fs'=8,'tp'=4] {'fs'}, dimensions={1} | all-to-all | bytes 1441792 | tf_op jit(solution)/shard_map/all_to_all | solution.py:53
  289.6 23.7 %all-gather.14.cloned.1.call-done = bf16[2048,704]{1,0:T(8,128)(2,1)} async-done(((bf16[512,704]{1,0:T(8,128)(2,1)}), bf16[2048,704]{1,0:T(8,128)(2,1)}) %all-gather.14.cloned.1.call-update) | async-done | bytes 2883600 | tf_op jit(solution)/shard_map/all_gather | solution.py:58
  313.3 3.9 copy.40
  317.2 26.1 %all-gather.16.cloned.1.call-done = bf16[2048,704]{1,0:T(8,128)(2,1)} async-done(((bf16[512,704]{1,0:T(8,128)(2,1)}), bf16[2048,704]{1,0:T(8,128)(2,1)}) %all-gather.16.cloned.1.call-update) | async-done | bytes 2883600 | tf_op jit(solution)/shard_map/all_gather | solution.py:59
  343.3 3.9 copy.43
  347.2 71.6 %all-gather.20.cloned.1.call-done = bf16[1024,2048]{1,0:T(8,128)(2,1)} async-done(((bf16[128,2048]{1,0:T(8,128)(2,1)}), bf16[1024,2048]{1,0:T(8,128)(2,1)}) %all-gather.20.cloned.1.call-update) | async-done | bytes 4194320 | tf_op jit(solution)/shard_map/all_gather | solution.py:83
  418.8 7.9 %fusion.16 = f32[1024,704]{0,1:T(8,128)} fusion(bf16[1024,2048]{1,0:T(8,128)(2,1)} %all-gather.20.cloned.1.call-done, bf16[2048,704]{1,0:T(8,128)(2,1)} %bitcast.60), kind=kOutput, calls=%fused_computation.27 | convolution fusion | flops 2952790016 | bytes 9961472 | tf_op jit(solution)/shard_map/dot_general | solution.py:14
  426.7 19.8 %all-gather.18.cloned.1.call-done = bf16[704,2048]{1,0:T(8,128)(2,1)} async-done(((bf16[704,512]{1,0:T(8,128)(2,1)}), bf16[704,2048]{1,0:T(8,128)(2,1)}) %all-gather.18.cloned.1.call-update) | async-done | bytes 2883600 | tf_op jit(solution)/shard_map/all_gather | solution.py:69
  446.5 12.2 %convolution_convert_fusion = bf16[1024,2048]{1,0:T(8,128)(2,1)} fusion(bf16[704,2048]{1,0:T(8,128)(2,1)} %all-gather.18.cloned.1.call-done, f32[1024,704]{0,1:T(8,128)} %fusion.16, bf16[1024,2048]{1,0:T(8,128)(2,1)} %all-gather.20.cloned.1.call-done, bf16[2048,704]{1,0:T(8,128)(2,1)} %bitcast.62), kind=kOutput, calls=%fused_computation.5 | convolution fusion | flops 5912002560 | bytes 17039360 | tf_op jit(solution)/shard_map/dot_general | solution.py:86
  458.7 2.7 copy.44
  461.4 4.7 copy.45
  466.2 2.7 copy.46
  468.8 4.6 copy.47
  473.5 73.7 %reduce-scatter.5.cloned.1.call-done = bf16[128,2048]{1,0:T(8,128)(2,1)} async-done(((bf16[1024,2048]{1,0:T(8,128)(2,1)}), bf16[128,2048]{1,0:T(8,128)(2,1)}) %reduce-scatter.5.cloned.1.call-update) | async-done | bytes 524304 | tf_op jit(solution)/shard_map/reduce_scatter | solution.py:85
  549.2 3.9 copy.50
  (53 shorter events, 21.4 us)
Async XLA Ops:
  7.2 91.8 %all-gather.8.cloned.1.call-start = ((), (), s32[]{:S(2)}) async-start(), calls=%async_computation.10 | async-start | bytes 3932160 | tf_op jit(solution)/shard_map/all_gather | solution.py:56
  51.3 70.3 %all-gather.10.cloned.1.call-start = ((), (), s32[]{:S(2)}) async-start(), calls=%async_computation.11 | async-start | bytes 3932160 | tf_op jit(solution)/shard_map/all_gather | solution.py:57
  70.7 24.0 %copy-start.5 = (f32[704,512]{1,0:T(8,128)S(1)}, f32[704,512]{1,0:T(8,128)}, u32[]{:S(2)}) copy-start(f32[704,512]{1,0:T(8,128)} %param.13) | copy-start | bytes 4325380
  94.7 56.0 %all-gather.12.cloned.1.call-start = ((), (), s32[]{:S(2)}) async-start(), calls=%async_computation.12 | async-start | bytes 3604480 | tf_op jit(solution)/shard_map/all_gather | solution.py:68
  95.8 188.1 %reduce-scatter.3.cloned.1.call-start = ((), (), s32[]{:S(2)}) async-start(), calls=%async_computation.16 | async-start | bytes 4718592 | tf_op jit(solution)/shard_map/reduce_scatter | solution.py:75
  121.5 4.1 copy-start.1
  163.3 0.7 copy-start.6
  163.3 150.0 %all-gather.14.cloned.1.call-start = ((), (), s32[]{:S(2)}) async-start(), calls=%async_computation.13 | async-start | bytes 3932160 | tf_op jit(solution)/shard_map/all_gather | solution.py:58
  224.2 119.1 %all-gather.16.cloned.1.call-start = ((), (), s32[]{:S(2)}) async-start(), calls=%async_computation.14 | async-start | bytes 3932160 | tf_op jit(solution)/shard_map/all_gather | solution.py:59
  283.4 135.4 %all-gather.20.cloned.1.call-start = ((), (), s32[]{:S(2)}) async-start(), calls=%async_computation.17 | async-start | bytes 4718592 | tf_op jit(solution)/shard_map/all_gather | solution.py:83
  285.4 0.8 copy-start.2
  287.2 159.4 %all-gather.18.cloned.1.call-start = ((), (), s32[]{:S(2)}) async-start(), calls=%async_computation.15 | async-start | bytes 3604480 | tf_op jit(solution)/shard_map/all_gather | solution.py:69
  289.5 257.7 %reduce-scatter.5.cloned.1.call-start = ((), (), s32[]{:S(2)}) async-start(), calls=%async_computation.18 | async-start | bytes 4718592 | tf_op jit(solution)/shard_map/reduce_scatter | solution.py:85
  461.4 4.7 copy-start
  468.8 78.4 %copy-start.3 = (bf16[128,2048]{1,0:T(8,128)(2,1)S(1)}, bf16[128,2048]{1,0:T(8,128)(2,1)}, u32[]{:S(2)}) copy-start(bf16[128,2048]{1,0:T(8,128)(2,1)} %copy-done.2) | copy-start | bytes 1572868
  549.2 3.9 copy-start.4
Sparse Core Ops, SparseCore 0:
  51.4 31.6 all-gather.7
  94.9 26.6 all-gather.9
  123.7 27.0 all-gather.11
  163.4 120.3 reduce-scatter.2
  285.3 28.0 all-gather.13
  314.7 28.4 all-gather.15
  346.0 72.7 all-gather.19
  420.9 25.5 all-gather.17
  458.9 88.2 reduce-scatter.4
where the time goes:
time: 562 us; the launch traced here: 561 us
  waiting for transfers between devices  256 us (46%)
  blocking collectives  189 us (34%)
  local copies, waits for them, and re-layouts  48.3 us (9%)
  matrix products  37.7 us (7%)
  other arithmetic  15.8 us (3%)
  between operations  14 us (2%)
    reduce_scatter x1, waiting for transfers between devices, per_device(): lax.psum_scatter(jnp.dot(selected, down_b, preferred_element_type=jnp.flo...  73.7 us
    all_gather x1, waiting for transfers between devices, per_device(): lax.all_gather(normalize(middle), 'fs', axis=0, tiled=True)  71.6 us
    all_to_all x1, blocking collectives, per_device(): lax.all_to_all(sliced[3], 'fs', split_axis=1, concat_axis=0, tiled=True)  39.6 us
    all_to_all x1, blocking collectives, per_device(): lax.all_to_all(sliced[2], 'fs', split_axis=1, concat_axis=0, tiled=True)  38.9 us
    all_gather x1, waiting for transfers between devices, per_device(): lax.all_gather(blocked[3], 'tp', axis=0, tiled=True)  26.1 us
    all_to_all x1, blocking collectives, per_device(): lax.all_to_all(sliced[0], 'fs', split_axis=1, concat_axis=0, tiled=True)  25.8 us
    all_gather x1, waiting for transfers between devices, per_device(): lax.all_gather(blocked[2], 'tp', axis=0, tiled=True)  23.7 us
    all_to_all x1, blocking collectives, per_device(): lax.all_to_all(sliced[1], 'fs', split_axis=1, concat_axis=0, tiled=True)  23.3 us
  transfers between devices with their start and end apart: 9, of which 8 were waited for; matrix products, arithmetic and copies ran while one was open for 11% of the time, Pallas kernels for 0%

commit v1 on v0

--- a/solution.py
+++ b/solution.py
@@ -80,7 +80,13 @@
     ).astype(jnp.float32)
     own_rows = lax.dynamic_slice_in_dim(tokens_in, lax.axis_index("fs") * share, share, 0)
     middle = (own_rows.astype(jnp.float32) + 0.5 * summed).astype(jnp.bfloat16)
-    act_second = activate(lax.all_gather(normalize(middle), "fs", axis=0, tiled=True), gate_b, up_b)
+    act_second = activate(
+        jnp.concatenate(
+            lax.all_to_all(jnp.stack([normalize(middle)] * lax.axis_size("fs")), "fs", 0, 0), axis=0
+        ),
+        gate_b,
+        up_b,
+    )
     selected = act_second
     final_sum = lax.psum_scatter(
         jnp.dot(selected, down_b, preferred_element_type=jnp.float32).astype(jnp.bfloat16),

time: 562 us -> 510 us (0.907)
  blocking collectives: 189 us -> 150 us
  waiting for transfers between devices: 256 us -> 231 us
  starting transfers between devices: 0.55 us -> 9.32 us
    all_to_all x0 -> x2, waiting for transfers between devices: none -> 74.6 us  [the longest x1 40.1 us: per_device(): lax.all_to_all(jnp.stack([normalize(middle)] * lax.axis_size('fs')), 'fs'...]
    all_gather x1 -> x0, waiting for transfers between devices: 71.6 us -> none  [per_device(): lax.all_gather(normalize(middle), 'fs', axis=0, tiled=True)]
    all_to_all x1 -> x0, blocking collectives: 39.6 us -> none  [per_device(): lax.all_to_all(sliced[3], 'fs', split_axis=1, concat_axis=0, tiled=True)]
    all_gather x1, waiting for transfers between devices: 19.8 us -> 0.01 us  [per_device(): lax.all_gather(round_down_b, 'tp', axis=1, tiled=True)]
    all_to_all x0 -> x2, starting transfers between devices: none -> 8.81 us  [the longest x1 4.6 us: per_device(): lax.all_to_all(jnp.stack([normalize(middle)] * lax.axis_size('fs')), 'fs'...]
    all_gather x1, waiting for transfers between devices: 23.7 us -> 17.2 us  [per_device(): lax.all_gather(blocked[2], 'tp', axis=0, tiled=True)]
  transfers between devices with their start and end apart: 9 -> 10, of which waited for: 8 -> 7; matrix products, arithmetic and copies ran while one was open for 11% -> 12% of each run, Pallas kernels for 0% -> 0%
where the time goes in v1:
time: 510 us; the launch traced here: 509 us
  waiting for transfers between devices  231 us (45%)
  blocking collectives  150 us (29%)
  local copies, waits for them, and re-layouts  51.7 us (10%)
  matrix products  37.7 us (7%)
  other arithmetic  15 us (3%)
  between operations  14.3 us (3%)
  starting transfers between devices  9.32 us (2%)
    reduce_scatter x1, waiting for transfers between devices, per_device(): lax.psum_scatter(jnp.dot(selected, down_b, preferred_element_type=jnp.flo...  72.7 us
    all_to_all x1, waiting for transfers between devices, per_device(): lax.all_to_all(jnp.stack([normalize(middle)] * lax.axis_size('fs')), 'fs'...  40.1 us
    all_to_all x1, blocking collectives, per_device(): lax.all_to_all(sliced[2], 'fs', split_axis=1, concat_axis=0, tiled=True)  38.9 us
    all_to_all x1, waiting for transfers between devices, per_device(): lax.all_to_all(sliced[3], 'fs', split_axis=1, concat_axis=0, tiled=True)  34.5 us
    all_gather x1, waiting for transfers between devices, per_device(): lax.all_gather(blocked[3], 'tp', axis=0, tiled=True)  26.1 us
    all_to_all x1, blocking collectives, per_device(): lax.all_to_all(sliced[0], 'fs', split_axis=1, concat_axis=0, tiled=True)  25.8 us
    all_to_all x1, blocking collectives, per_device(): lax.all_to_all(sliced[1], 'fs', split_axis=1, concat_axis=0, tiled=True)  23.3 us
    unnamed x20, local copies, waits for them, and re-layouts  21.5 us
  transfers between devices with their start and end apart: 10, of which 7 were waited for; matrix products, arithmetic and copies ran while one was open for 12% of the time, Pallas kernels for 0%

profile of v1, /device:TPU:0, one launch (start us, length us, event | category | flops | bytes accessed | tf_op | source)
XLA Modules:
  0.0 508.6 jit_solution(13658312802603450785)
XLA Ops:
  9.3 15.0 %all_to_all.145 = bf16[4,64,1408]{2,1,0:T(8,128)(2,1)S(1)} all-to-all(bf16[4,64,1408]{2,1,0:T(8,128)(2,1)S(1)} %bitcast.74), channel_id=1, replica_groups=mesh['fs'=8,'tp'=4] {'tp'}, dimensions={0} | all-to-all | bytes 1441792 | tf_op jit(solution)/shard_map/all_to_all | solution.py:44
  25.5 25.8 %all_to_all.146 = bf16[64,8,704]{2,0,1:T(8,128)(2,1)} all-to-all(bf16[64,8,704]{2,0,1:T(8,128)(2,1)S(1)} %copy.33), channel_id=1, replica_groups=mesh['fs'=8,'tp'=4] {'fs'}, dimensions={1} | all-to-all | bytes 1441792 | tf_op jit(solution)/shard_map/all_to_all | solution.py:50
  51.3 18.9 %all_to_all.147 = bf16[4,64,1408]{2,1,0:T(8,128)(2,1)S(1)} all-to-all(bf16[4,64,1408]{2,1,0:T(8,128)(2,1)S(1)} %bitcast.72), channel_id=1, replica_groups=mesh['fs'=8,'tp'=4] {'tp'}, dimensions={0} | all-to-all | bytes 1441792 | tf_op jit(solution)/shard_map/all_to_all | solution.py:45
  71.4 23.3 %all_to_all.148 = bf16[64,8,704]{2,0,1:T(8,128)(2,1)} all-to-all(bf16[64,8,704]{2,0,1:T(8,128)(2,1)S(1)} %copy.36), channel_id=1, replica_groups=mesh['fs'=8,'tp'=4] {'fs'}, dimensions={1} | all-to-all | bytes 1441792 | tf_op jit(solution)/shard_map/all_to_all | solution.py:51
  95.8 3.1 fusion
  98.9 2.5 copy.34
  101.4 20.1 %all-gather.9.cloned.1.call-done = bf16[2048,704]{1,0:T(8,128)(2,1)} async-done(((bf16[512,704]{1,0:T(8,128)(2,1)}), bf16[2048,704]{1,0:T(8,128)(2,1)}) %all-gather.9.cloned.1.call-update) | async-done | bytes 2883600 | tf_op jit(solution)/shard_map/all_gather | solution.py:57
  121.5 4.1 copy.37
  125.6 5.0 fusion.4
  130.6 20.1 %all-gather.11.cloned.1.call-done = bf16[704,2048]{1,0:T(8,128)(2,1)} async-done(((bf16[704,512]{1,0:T(8,128)(2,1)}), bf16[704,2048]{1,0:T(8,128)(2,1)}) %all-gather.11.cloned.1.call-update) | async-done | bytes 2883600 | tf_op jit(solution)/shard_map/all_gather | solution.py:68
  150.7 12.6 %convolution_convert_fusion.1 = bf16[1024,2048]{1,0:T(8,128)(2,1)} fusion(bf16[704,2048]{1,0:T(8,128)(2,1)} %all-gather.11.cloned.1.call-done, f32[1024,704]{0,1:T(8,128)} %fusion.4, bf16[2048,704]{1,0:T(8,128)(2,1)} %bitcast.59, bf16[1,1024,2048]{2,1,0:T(8,128)(2,1)} %param.9, f32[1024]{0:T(1024)S(1)} %add_rsqrt_fusion), kind=kOutput, calls=%fused_computation.6 | convolution fusion | flops 5918294016 | bytes 17043456 | tf_op jit(solution)/shard_map/dot_general | solution.py:76
  164.0 2.9 multiply_convert_fusion.2
  166.9 13.3 %all_to_all.149 = bf16[4,64,1408]{2,1,0:T(8,128)(2,1)S(1)} all-to-all(bf16[4,64,1408]{2,1,0:T(8,128)(2,1)S(1)} %bitcast.75), channel_id=1, replica_groups=mesh['fs'=8,'tp'=4] {'tp'}, dimensions={0} | all-to-all | bytes 1441792 | tf_op jit(solution)/shard_map/all_to_all | solution.py:46
  185.3 38.9 %all_to_all.150 = bf16[64,8,704]{2,0,1:T(8,128)(2,1)} all-to-all(bf16[64,8,704]{2,0,1:T(8,128)(2,1)S(1)} %copy.39), channel_id=1, replica_groups=mesh['fs'=8,'tp'=4] {'fs'}, dimensions={1} | all-to-all | bytes 1441792 | tf_op jit(solution)/shard_map/all_to_all | solution.py:52
  224.2 14.4 %all_to_all.151 = bf16[4,64,1408]{2,1,0:T(8,128)(2,1)S(1)} all-to-all(bf16[4,64,1408]{2,1,0:T(8,128)(2,1)} %bitcast.73), channel_id=1, replica_groups=mesh['fs'=8,'tp'=4] {'tp'}, dimensions={0} | all-to-all | bytes 1441792 | tf_op jit(solution)/shard_map/all_to_all | solution.py:47
  244.6 4.2 all-to-all-start.7
  248.9 34.5 %all-to-all-done.7 = bf16[64,8,704]{2,0,1:T(8,128)(2,1)} async-done(((bf16[64,8,704]{2,0,1:T(8,128)(2,1)}), bf16[64,8,704]{2,0,1:T(8,128)(2,1)}, u32[]{:S(2)}, u32[]{:S(2)}) %all-to-all-start.7) | async-done | bytes 720928 | tf_op jit(solution)/shard_map/all_to_all | solution.py:53
  286.0 2.6 stack.2
  288.5 4.6 all-to-all-start.8
  295.5 17.2 %all-gather.13.cloned.1.call-done = bf16[2048,704]{1,0:T(8,128)(2,1)} async-done(((bf16[512,704]{1,0:T(8,128)(2,1)}), bf16[2048,704]{1,0:T(8,128)(2,1)}) %all-gather.13.cloned.1.call-update) | async-done | bytes 2883600 | tf_op jit(solution)/shard_map/all_gather | solution.py:58
  312.8 3.8 copy.40
  316.6 26.1 %all-gather.15.cloned.1.call-done = bf16[2048,704]{1,0:T(8,128)(2,1)} async-done(((bf16[512,704]{1,0:T(8,128)(2,1)}), bf16[2048,704]{1,0:T(8,128)(2,1)}) %all-gather.15.cloned.1.call-update) | async-done | bytes 2883600 | tf_op jit(solution)/shard_map/all_gather | solution.py:59
  342.7 3.9 copy.43
  346.6 40.1 %all-to-all-done.8 = bf16[8,128,2048]{2,1,0:T(8,128)(2,1)} async-done(((bf16[8,128,2048]{2,1,0:T(8,128)(2,1)}), bf16[8,128,2048]{2,1,0:T(8,128)(2,1)}, u32[]{:S(2)}, u32[]{:S(2)}) %all-to-all-start.8) | async-done | bytes 4194336 | tf_op jit(solution)/shard_map/all_to_all | solution.py:85
  386.7 7.9 %fusion.16 = f32[1024,704]{0,1:T(8,128)} fusion(bf16[1024,2048]{1,0:T(8,128)(2,1)} %bitcast.30, bf16[2048,704]{1,0:T(8,128)(2,1)} %bitcast.61), kind=kOutput, calls=%fused_computation.27 | convolution fusion | flops 2952790016 | bytes 9961472 | tf_op jit(solution)/shard_map/dot_general | solution.py:14
  394.6 12.2 %convolution_convert_fusion = bf16[1024,2048]{1,0:T(8,128)(2,1)} fusion(bf16[704,2048]{1,0:T(8,128)(2,1)} %all-gather.17.cloned.1.call-done, f32[1024,704]{0,1:T(8,128)} %fusion.16, bf16[1024,2048]{1,0:T(8,128)(2,1)} %bitcast.30, bf16[2048,704]{1,0:T(8,128)(2,1)} %bitcast.63), kind=kOutput, calls=%fused_computation.5 | convolution fusion | flops 5912002560 | bytes 17039360 | tf_op jit(solution)/shard_map/dot_general | solution.py:92
  406.8 2.7 copy.44
  409.5 4.7 copy.45
  414.3 2.7 copy.46
  417.0 4.6 copy.47
  421.6 72.7 %reduce-scatter.5.cloned.1.call-done = bf16[128,2048]{1,0:T(8,128)(2,1)} async-done(((bf16[1024,2048]{1,0:T(8,128)(2,1)}), bf16[128,2048]{1,0:T(8,128)(2,1)}) %reduce-scatter.5.cloned.1.call-update) | async-done | bytes 524304 | tf_op jit(solution)/shard_map/reduce_scatter | solution.py:91
  496.2 3.9 copy.50
  (54 shorter events, 25.9 us)
Async XLA Ops:
  7.2 91.8 %all-gather.7.cloned.1.call-start = ((), (), s32[]{:S(2)}) async-start(), calls=%async_computation.11 | async-start | bytes 3932160 | tf_op jit(solution)/shard_map/all_gather | solution.py:56
  51.3 70.3 %all-gather.9.cloned.1.call-start = ((), (), s32[]{:S(2)}) async-start(), calls=%async_computation.12 | async-start | bytes 3932160 | tf_op jit(solution)/shard_map/all_gather | solution.py:57
  70.7 24.0 %copy-start.5 = (f32[704,512]{1,0:T(8,128)S(1)}, f32[704,512]{1,0:T(8,128)}, u32[]{:S(2)}) copy-start(f32[704,512]{1,0:T(8,128)} %param.13) | copy-start | bytes 4325380
  94.7 56.0 %all-gather.11.cloned.1.call-start = ((), (), s32[]{:S(2)}) async-start(), calls=%async_computation.13 | async-start | bytes 3604480 | tf_op jit(solution)/shard_map/all_gather | solution.py:68
  95.8 187.7 %reduce-scatter.3.cloned.1.call-start = ((), (), s32[]{:S(2)}) async-start(), calls=%async_computation.17 | async-start | bytes 4718592 | tf_op jit(solution)/shard_map/reduce_scatter | solution.py:75
  121.5 4.1 copy-start.1
  163.3 0.7 copy-start.6
  163.3 149.4 %all-gather.13.cloned.1.call-start = ((), (), s32[]{:S(2)}) async-start(), calls=%async_computation.14 | async-start | bytes 3932160 | tf_op jit(solution)/shard_map/all_gather | solution.py:58
  244.6 38.8 %all-to-all-start.7 = ((bf16[64,8,704]{2,0,1:T(8,128)(2,1)}), bf16[64,8,704]{2,0,1:T(8,128)(2,1)}, u32[]{:S(2)}, u32[]{:S(2)}) async-start(bf16[64,8,704]{2,0,1:T(8,128)(2,1)} %copy.42), calls=%async_computation.7 | async-start | bytes 1572864 | tf_op jit(solution)/shard_map/all_to_all | solution.py:53
  248.8 93.9 %all-gather.15.cloned.1.call-start = ((), (), s32[]{:S(2)}) async-start(), calls=%async_computation.15 | async-start | bytes 3932160 | tf_op jit(solution)/shard_map/all_gather | solution.py:59
  285.0 0.8 copy-start.2
  288.5 98.2 %all-to-all-start.8 = ((bf16[8,128,2048]{2,1,0:T(8,128)(2,1)}), bf16[8,128,2048]{2,1,0:T(8,128)(2,1)}, u32[]{:S(2)}, u32[]{:S(2)}) async-start(bf16[8,128,2048]{2,1,0:T(8,128)(2,1)} %stack.2), calls=%async_computation.9 | async-start | bytes 8388608 | tf_op jit(solution)/shard_map/all_to_all | solution.py:85
  293.1 101.5 %all-gather.17.cloned.1.call-start = ((), (), s32[]{:S(2)}) async-start(), calls=%async_computation.16 | async-start | bytes 3604480 | tf_op jit(solution)/shard_map/all_gather | solution.py:69
  295.5 198.8 %reduce-scatter.5.cloned.1.call-start = ((), (), s32[]{:S(2)}) async-start(), calls=%async_computation.18 | async-start | bytes 4718592 | tf_op jit(solution)/shard_map/reduce_scatter | solution.py:91
  409.5 4.7 copy-start
  417.0 77.3 %copy-start.3 = (bf16[128,2048]{1,0:T(8,128)(2,1)S(1)}, bf16[128,2048]{1,0:T(8,128)(2,1)}, u32[]{:S(2)}) copy-start(bf16[128,2048]{1,0:T(8,128)(2,1)} %copy-done.2) | copy-start | bytes 1572868
  496.2 3.9 copy-start.4
Sparse Core Ops, SparseCore 0:
  51.4 31.6 all-gather.6
  94.9 26.6 all-gather.8
  123.7 27.0 all-gather.10
  163.4 119.4 reduce-scatter.2
  284.3 28.4 all-gather.12
  314.2 28.4 all-gather.14
  344.8 27.0 all-gather.16
  407.0 87.2 reduce-scatter.4
